TPU v7x, 32 devices: a whole 2x2x4 slice. The times are simulated.
32 devices in a mesh: grp: 2 (over y), sp: 4 (over z), dp: 4 (over x, core).
Axes of the slice: x: 2, y: 2, z: 4, core: 2. Of those that a mesh axis runs over, the one named last changes fastest.
Arguments:
- activations: bfloat16 [8, 2048, 2048], P(('grp', 'dp'), 'sp'), parts along dimension 0, may hold values from -6 to 6
- value_weight: bfloat16 [2048, 1024], P('sp', 'dp'), may hold values from -0.125 to 0.125
- gate_weight: bfloat16 [2048, 1024], P('sp', 'dp'), may hold values from -0.125 to 0.125
- conv_taps: float32 [31, 1024], replicated, may hold values from -4 to 4
- conv_bias: float32 [1024], replicated, may hold values from -3 to 3
- norm_gain: float32 [1024], replicated, may hold values from 0.1 to 1.9
- norm_bias: float32 [1024], replicated, may hold values from -3 to 3
- out_weight: bfloat16 [1024, 2048], P('sp', 'dp'), may hold values from -0.1875 to 0.1875
Outputs:
- mixed_out: bfloat16 [8, 2048, 2048], P(('grp', 'dp'), 'sp'), parts along dimension 0
There are 2 independent parts, one for each index of `grp`. A program takes and returns all parts, laid end to end along the dimension named above; an argument that names none is the same for every part. Nothing has to cross between parts.
All inputs are finite; a program needn't handle non-finite values.
Results may differ from a plain program's by a relative error of at most 0.013.
Values may be sent and summed in bfloat16 or wider, within the bound.
A program may use at most 64 MiB of HBM per device.

v0:
```python
import jax
import jax.numpy as jnp
from jax import lax
from jax.sharding import PartitionSpec as P

epsilon = 1e-05


def passed_along(value, axis, steps):
    count = lax.axis_size(axis)
    first, last = (max(0, -steps), min(count, count - steps))
    return lax.ppermute(value, axis, [(source, source + steps) for source in range(first, last)])


def local(
    activations, value_weight, gate_weight, conv_taps, conv_bias, norm_gain, norm_bias, out_weight
):
    tokens = activations[0]
    tok_rows = tokens.shape[0]
    kernel_len = conv_taps.shape[0]
    whole_value, whole_gate = (
        lax.all_gather(value_weight, "sp", axis=0, tiled=True),
        lax.all_gather(gate_weight, "sp", axis=0, tiled=True),
    )
    stacked = jnp.stack([whole_value, whole_gate], axis=0)
    both_rows = jnp.einsum(
        "td,kdc->ktc",
        tokens,
        lax.all_gather(stacked, "dp", axis=2, tiled=True),
        preferred_element_type=jnp.float32,
    )
    value_rows = both_rows[0]
    gate_rows = both_rows[1]
    value_half = value_rows.astype(jnp.bfloat16)
    gate_half = gate_rows.astype(jnp.bfloat16)
    gated_rows = (
        value_half.astype(jnp.float32) * jax.nn.sigmoid(gate_half.astype(jnp.float32))
    ).astype(jnp.bfloat16)
    prior = passed_along(gated_rows[tok_rows - (kernel_len - 1) :], "sp", 1)
    padded = jnp.concatenate([prior, gated_rows], axis=0).astype(jnp.float32)
    conv_sum = jnp.zeros(gated_rows.shape, jnp.float32) + conv_bias[None, :]
    for tap_index in range(kernel_len):
        conv_sum = (
            conv_sum + conv_taps[tap_index][None, :] * padded[tap_index : tap_index + tok_rows]
        )
    mean_row = jnp.mean(conv_sum, axis=-1, keepdims=True)
    centered = conv_sum - mean_row
    spread = jnp.mean(centered * centered, axis=-1, keepdims=True)
    normed = centered * lax.rsqrt(spread + epsilon) * norm_gain[None, :] + norm_bias[None, :]
    swished = jax.nn.silu(normed).astype(jnp.bfloat16)
    whole_output = lax.all_gather(out_weight, "sp", axis=0, tiled=True)
    result = jnp.dot(
        swished,
        lax.all_gather(whole_output, "dp", axis=1, tiled=True),
        preferred_element_type=jnp.float32,
    )
    return result.astype(jnp.bfloat16)[None]


def solution(mesh):
    in_specs = (
        P(("grp", "dp"), "sp", None),
        P("sp", "dp"),
        P("sp", "dp"),
        P(),
        P(),
        P(),
        P(),
        P("sp", "dp"),
    )
    out_specs = P(("grp", "dp"), "sp", None)
    return jax.shard_map(local, mesh=mesh, in_specs=in_specs, out_specs=out_specs, check_vma=False)
```

profile of v0, /device:TPU:0, one launch (start us, length us, event | category | flops | bytes accessed | tf_op | source)
XLA Modules:
  0.0 207.2 jit_solution(12494679978274099827)
XLA Ops:
  6.5 0.7 all-gather.6.cloned.1.call-update
  7.3 0.0 all-gather.8.cloned.1.call-start
  7.3 0.7 all-gather.8.cloned.1.call-update
  8.0 0.0 all-gather.12.cloned.1.call-start
  8.1 0.7 all-gather.12.cloned.1.call-update
  8.7 0.0 all-gather.10.cloned.1.call-start
  8.8 30.9 %all-gather.6.cloned.1.call-done = bf16[2048,256]{1,0:T(8,128)(2,1)} async-done(((bf16[512,256]{1,0:T(8,128)(2,1)}), bf16[2048,256]{1,0:T(8,128)(2,1)}) %all-gather.6.cloned.1.call-update) | async-done | bytes 1048592 | tf_op jit(solution)/shard_map/all_gather | solution.py:22
  39.6 29.0 %all-gather.8.cloned.1.call-done = bf16[2048,256]{1,0:T(8,128)(2,1)} async-done(((bf16[512,256]{1,0:T(8,128)(2,1)}), bf16[2048,256]{1,0:T(8,128)(2,1)}) %all-gather.8.cloned.1.call-update) | async-done | bytes 1048592 | tf_op jit(solution)/shard_map/all_gather | solution.py:23
  68.6 3.1 %pad_maximum_fusion = bf16[2,2048,256]{2,1,0:T(8,128)(2,1)} fusion(bf16[1,2048,256]{2,1,0:T(8,128)(2,1)} %bitcast.50, bf16[1,2048,256]{2,1,0:T(8,128)(2,1)} %bitcast.49), kind=kLoop, calls=%fused_computation.64 | loop fusion | flops 1048576 | bytes 4194304 | tf_op jit(solution)/shard_map/stack | solution.py:25
  71.7 0.0 all-gather.10.cloned.1.call-update
  71.7 0.0 all-gather.14.cloned.1.call-start
  71.7 25.8 %all-gather.12.cloned.1.call-done = bf16[1024,512]{1,0:T(8,128)(2,1)} async-done(((bf16[256,512]{1,0:T(8,128)(2,1)}), bf16[1024,512]{1,0:T(8,128)(2,1)}) %all-gather.12.cloned.1.call-update) | async-done | bytes 1048592 | tf_op jit(solution)/shard_map/all_gather | solution.py:51
  97.6 0.0 all-gather.14.cloned.1.call-update
  97.6 0.0 copy-done.2
  97.6 0.1 fusion.44
  97.7 60.0 %all-gather.10.cloned.1.call-done = bf16[2,2048,1024]{2,1,0:T(8,128)(2,1)} async-done(((bf16[2,2048,256]{2,1,0:T(8,128)(2,1)}), bf16[2,2048,1024]{2,1,0:T(8,128)(2,1)}) %all-gather.10.cloned.1.call-update) | async-done | bytes 8388624 | tf_op jit(solution)/shard_map/all_gather | solution.py:29
  157.8 0.0 copy-done
  157.8 8.1 %convert_bitcast_fusion = bf16[2,512,1024]{2,1,0:T(8,128)(2,1)S(1)} fusion(bf16[2,2048,1024]{2,1,0:T(8,128)(2,1)} %all-gather.10.cloned.1.call-done, bf16[1,512,2048]{2,1,0:T(8,128)(2,1)S(1)} %copy-done), kind=kOutput, calls=%fused_computation.68 | convolution fusion | flops 4296015872 | bytes 12582912 | tf_op jit(solution)/shard_map/td,kdc->ktc/dot_general | solution.py:26
  165.8 0.6 multiply_convert_fusion
  166.5 3.4 %collective-permute-start = (bf16[30,1024]{1,0:T(8,128)(2,1)S(1)}, bf16[30,1024]{1,0:T(8,128)(2,1)S(1)}, u32[]{:S(2)}, u32[]{:S(2)}) collective-permute-start(bf16[30,1024]{1,0:T(8,128)(2,1)S(1)} %slice_bitcast_fusion), channel_id=1, source_target_pairs={{0,4},{4,8},{8,12},{1,5},{5,9},{9,13},{2,6},{6,10},{10,14},{3,7},{... | collective-permute-start | bytes 184328 | tf_op jit(solution)/shard_map/ppermute | solution.py:12
  169.9 0.6 fusion.48
  170.5 0.0 copy-start.3
  170.5 1.3 collective-permute-done
  171.8 0.3 maximum_convert_fusion
  172.1 9.8 %fusion.42 = (f32[512]{0:T(512)S(1)}, f32[512,1024]{1,0:T(8,128)S(1)}) fusion(f32[542,1024]{1,0:T(8,128)S(1)} %maximum_convert_fusion, f32[1024]{0:T(1024)S(1)} %bitcast.61, f32[1024]{0:T(1024)S(1)} %bitcast.62, f32[1024]{0:T(1024)S(1)} %bitcast.64, f32[1024]{0:T(1024)S(1)} %bitcast.65, f32[1024]{0:T(1024)S(1)} %bitcast.66, f32[1024]{0:T(1024)S(1)} %bitcast.67, ...), kind=kLoop, calls=%fused_computation.81 | loop fusion | flops 33029632 | bytes 67241984 | tf_op jit(solution)/shard_map/reduce_sum | solution.py:46
  181.9 0.0 copy-start.4
  181.9 0.0 copy-start.5
  182.0 1.3 copy-done.1
  183.3 0.3 multiply_reduce_fusion
  183.6 10.0 %all-gather.14.cloned.1.call-done = bf16[1024,2048]{1,0:T(8,128)(2,1)} async-done(((bf16[1024,512]{1,0:T(8,128)(2,1)}), bf16[1024,2048]{1,0:T(8,128)(2,1)}) %all-gather.14.cloned.1.call-update) | async-done | bytes 4194320 | tf_op jit(solution)/shard_map/all_gather | solution.py:54
  193.7 0.0 copy-done.5
  193.7 7.0 %fusion = bf16[1,512,2048]{2,1,0:T(8,128)(2,1)} fusion(bf16[1024,2048]{1,0:T(8,128)(2,1)} %all-gather.14.cloned.1.call-done, f32[512,1024]{1,0:T(8,128)} %copy-done.1, f32[1024]{0:T(1024)S(1)} %copy-done.4, f32[1024]{0:T(1024)S(1)} %copy-done.5, f32[512]{0:T(512)S(1)} %add_rsqrt_fusion, f32[512]{0:T(512)S(1)} %broadcast_multiply_fusion), kind=kOutput, calls=%fused_computation.1 | convolution fusion | flops 2153250816 | bytes 8400896 | tf_op jit(solution)/shard_map/dot_general | solution.py:52
  (10 shorter events, 0.1 us)
Async XLA Ops:
  6.5 151.2 %copy-start = (bf16[1,512,2048]{2,1,0:T(8,128)(2,1)S(1)}, bf16[1,512,2048]{2,1,0:T(8,128)(2,1)}, u32[]{:S(2)}) copy-start(bf16[1,512,2048]{2,1,0:T(8,128)(2,1)} %param.8) | copy-start | bytes 6291460
  6.5 33.1 %all-gather.6.cloned.1.call-start = ((), (), s32[]{:S(2)}) async-start(), calls=%async_computation | async-start | bytes 1310720 | tf_op jit(solution)/shard_map/all_gather | solution.py:22
  7.3 61.3 %all-gather.8.cloned.1.call-start = ((), (), s32[]{:S(2)}) async-start(), calls=%async_computation.1 | async-start | bytes 1310720 | tf_op jit(solution)/shard_map/all_gather | solution.py:23
  8.0 89.6 %all-gather.12.cloned.1.call-start = ((), (), s32[]{:S(2)}) async-start(), calls=%async_computation.3 | async-start | bytes 1310720 | tf_op jit(solution)/shard_map/all_gather | solution.py:51
  8.7 149.0 %all-gather.10.cloned.1.call-start = ((), (), s32[]{:S(2)}) async-start(), calls=%async_computation.2 | async-start | bytes 10485760 | tf_op jit(solution)/shard_map/all_gather | solution.py:29
  71.7 25.9 %copy-start.2 = (f32[31,1024]{1,0:T(8,128)S(1)}, f32[31,1024]{1,0:T(8,128)}, u32[]{:S(2)}) copy-start(f32[31,1024]{1,0:T(8,128)} %param.11) | copy-start | bytes 380932
  71.7 122.0 %all-gather.14.cloned.1.call-start = ((), (), s32[]{:S(2)}) async-start(), calls=%async_computation.4 | async-start | bytes 5242880 | tf_op jit(solution)/shard_map/all_gather | solution.py:54
  166.5 5.3 %collective-permute-start = (bf16[30,1024]{1,0:T(8,128)(2,1)S(1)}, bf16[30,1024]{1,0:T(8,128)(2,1)S(1)}, u32[]{:S(2)}, u32[]{:S(2)}) collective-permute-start(bf16[30,1024]{1,0:T(8,128)(2,1)S(1)} %slice_bitcast_fusion), channel_id=1, source_target_pairs={{0,4},{4,8},{8,12},{1,5},{5,9},{9,13},{2,6},{6,10},{10,14},{3,7},{... | collective-permute-start | bytes 184328 | tf_op jit(solution)/shard_map/ppermute | solution.py:12
  170.5 1.6 copy-start.3
  181.9 1.3 copy-start.1
  181.9 11.7 %copy-start.4 = (f32[1024]{0:T(1024)S(1)}, f32[1024]{0:T(1024)}, u32[]{:S(2)}) copy-start(f32[1024]{0:T(1024)} %param.14) | copy-start | bytes 12292
  181.9 11.7 %copy-start.5 = (f32[1024]{0:T(1024)S(1)}, f32[1024]{0:T(1024)}, u32[]{:S(2)}) copy-start(f32[1024]{0:T(1024)} %param.13) | copy-start | bytes 12292
Sparse Core Ops, SparseCore 0:
  8.9 30.6 all-gather.5
  41.2 27.3 all-gather.7
  70.2 27.3 all-gather.11
  99.0 58.7 all-gather.9
  159.2 34.4 all-gather.13
where the time goes:
time: 207 us
  waiting for transfers between devices  159 us (77%)
  matrix products  15 us (7%)
  other arithmetic  14.7 us (7%)
  between operations  13.3 us (6%)
  starting transfers between devices  3.55 us (2%)
    all_gather x1, waiting for transfers between devices, local(): lax.all_gather(stacked, 'dp', axis=2, tiled=True)  60 us
    all_gather x1, waiting for transfers between devices, local(): lax.all_gather(value_weight, 'sp', axis=0, tiled=True)  30.9 us
    all_gather x1, waiting for transfers between devices, local(): lax.all_gather(gate_weight, 'sp', axis=0, tiled=True)  29 us
    all_gather x1, waiting for transfers between devices, local(): whole_output = lax.all_gather(out_weight, 'sp', axis=0, tiled=True)  25.8 us
    all_gather x1, waiting for transfers between devices, local(): lax.all_gather(whole_output, 'dp', axis=1, tiled=True)  10 us
    reduce_sum x1, other arithmetic, local(): mean_row = jnp.mean(conv_sum, axis=-1, keepdims=True)  9.83 us
    dot_general x1, matrix products, local(): jnp.einsum('td,kdc->ktc', tokens, lax.all_gather(stacked, 'dp', axis=2, t...  8.06 us
    dot_general x1, matrix products, local(): jnp.dot(swished, lax.all_gather(whole_output, 'dp', axis=1, tiled=True),...  6.96 us
  transfers between devices with their start and end apart: 6, of which 6 were waited for; matrix products, arithmetic and copies ran while one was open for 11% of the time, Pallas kernels for 0%

commit v1 on v0

--- a/solution.py
+++ b/solution.py
@@ -48,7 +48,12 @@
     spread = jnp.mean(centered * centered, axis=-1, keepdims=True)
     normed = centered * lax.rsqrt(spread + epsilon) * norm_gain[None, :] + norm_bias[None, :]
     swished = jax.nn.silu(normed).astype(jnp.bfloat16)
-    whole_output = lax.all_gather(out_weight, "sp", axis=0, tiled=True)
+    ring = [out_weight]
+    for hop in range(3):
+        ring.append(lax.ppermute(ring[-1], "sp", [(dev, (dev + 1) % 4) for dev in range(4)]))
+    whole_output = jnp.roll(
+        jnp.concatenate(ring[::-1], axis=0), (lax.axis_index("sp") + 1) * ring[0].shape[0], axis=0
+    )
     result = jnp.dot(
         swished,
         lax.all_gather(whole_output, "dp", axis=1, tiled=True),

time: 207 us -> 180 us (0.87)
  waiting for transfers between devices: 159 us -> 128 us
  local copies, waits for them, and re-layouts: 1.44 us -> 3.57 us
    all_gather x1, waiting for transfers between devices: 60 us -> 30.5 us  [local(): lax.all_gather(stacked, 'dp', axis=2, tiled=True)]
    all_gather x1 -> x0, waiting for transfers between devices: 25.8 us -> none  [local(): whole_output = lax.all_gather(out_weight, 'sp', axis=0, tiled=True)]
    ppermute x0 -> x3, waiting for transfers between devices: none -> 24.6 us  [local(): lax.ppermute(ring[-1], 'sp', [(dev, (dev + 1) % 4) for dev in range(4)])]
  transfers between devices with their start and end apart: 6 -> 8, of which waited for: 6 -> 8; matrix products, arithmetic and copies ran while one was open for 11% -> 12% of each run, Pallas kernels for 0% -> 0%
where the time goes in v1:
time: 180 us
  waiting for transfers between devices  128 us (71%)
  matrix products  15 us (8%)
  other arithmetic  14.7 us (8%)
  between operations  13.3 us (7%)
  starting transfers between devices  4.97 us (3%)
  local copies, waits for them, and re-layouts  3.57 us (2%)
    all_gather x1, waiting for transfers between devices, local(): lax.all_gather(value_weight, 'sp', axis=0, tiled=True)  31.6 us
    all_gather x1, waiting for transfers between devices, local(): lax.all_gather(stacked, 'dp', axis=2, tiled=True)  30.5 us
    all_gather x1, waiting for transfers between devices, local(): lax.all_gather(gate_weight, 'sp', axis=0, tiled=True)  29 us
    ppermute x3, waiting for transfers between devices, local(): lax.ppermute(ring[-1], 'sp', [(dev, (dev + 1) % 4) for dev in range(4)])  24.6 us
    all_gather x1, waiting for transfers between devices, local(): lax.all_gather(whole_output, 'dp', axis=1, tiled=True)  10.1 us
    reduce_sum x1, other arithmetic, local(): mean_row = jnp.mean(conv_sum, axis=-1, keepdims=True)  9.83 us
    dot_general x1, matrix products, local(): jnp.einsum('td,kdc->ktc', tokens, lax.all_gather(stacked, 'dp', axis=2, t...  8.07 us
    dot_general x1, matrix products, local(): jnp.dot(swished, lax.all_gather(whole_output, 'dp', axis=1, tiled=True),...  6.97 us
  transfers between devices with their start and end apart: 8, of which 8 were waited for; matrix products, arithmetic and copies ran while one was open for 12% of the time, Pallas kernels for 0%

profile of v1, /device:TPU:0, one launch (start us, length us, event | category | flops | bytes accessed | tf_op | source)
XLA Modules:
  0.0 180.0 jit_solution(5782916036457545505)
XLA Ops:
  6.5 0.7 all-gather.5.cloned.1.call-update
  7.3 0.0 all-gather.7.cloned.1.call-start
  7.3 0.7 all-gather.7.cloned.1.call-update
  8.0 0.0 all-gather.9.cloned.1.call-start
  8.1 31.6 %all-gather.5.cloned.1.call-done = bf16[2048,256]{1,0:T(8,128)(2,1)} async-done(((bf16[512,256]{1,0:T(8,128)(2,1)}), bf16[2048,256]{1,0:T(8,128)(2,1)}) %all-gather.5.cloned.1.call-update) | async-done | bytes 1048592 | tf_op jit(solution)/shard_map/all_gather | solution.py:22
  39.6 29.0 %all-gather.7.cloned.1.call-done = bf16[2048,256]{1,0:T(8,128)(2,1)} async-done(((bf16[512,256]{1,0:T(8,128)(2,1)}), bf16[2048,256]{1,0:T(8,128)(2,1)}) %all-gather.7.cloned.1.call-update) | async-done | bytes 1048592 | tf_op jit(solution)/shard_map/all_gather | solution.py:23
  68.6 3.1 %pad_maximum_fusion = bf16[2,2048,256]{2,1,0:T(8,128)(2,1)} fusion(bf16[1,2048,256]{2,1,0:T(8,128)(2,1)} %bitcast.50, bf16[1,2048,256]{2,1,0:T(8,128)(2,1)} %bitcast.49), kind=kLoop, calls=%fused_computation.64 | loop fusion | flops 1048576 | bytes 4194304 | tf_op jit(solution)/shard_map/stack | solution.py:25
  71.7 0.0 all-gather.9.cloned.1.call-update
  71.7 0.0 all-gather.11.cloned.1.call-start
  71.7 0.9 copy-done.2
  72.6 1.4 collective-permute-start.1
  74.1 7.9 %collective-permute-done.1 = bf16[256,512]{1,0:T(8,128)(2,1)S(1)} collective-permute-done((bf16[256,512]{1,0:T(8,128)(2,1)S(1)}, bf16[256,512]{1,0:T(8,128)(2,1)S(1)}, u32[]{:S(2)}, u32[]{:S(2)}) %collective-permute-start.1) | collective-permute-done | bytes 262176 | tf_op jit(solution)/shard_map/ppermute | solution.py:53
  82.0 8.5 %collective-permute-done.2 = bf16[256,512]{1,0:T(8,128)(2,1)S(1)} collective-permute-done((bf16[256,512]{1,0:T(8,128)(2,1)S(1)}, bf16[256,512]{1,0:T(8,128)(2,1)S(1)}, u32[]{:S(2)}, u32[]{:S(2)}) %collective-permute-start.2) | collective-permute-done | bytes 262176 | tf_op jit(solution)/shard_map/ppermute | solution.py:53
  90.5 8.2 %collective-permute-done.3 = bf16[256,512]{1,0:T(8,128)(2,1)S(1)} collective-permute-done((bf16[256,512]{1,0:T(8,128)(2,1)S(1)}, bf16[256,512]{1,0:T(8,128)(2,1)S(1)}, u32[]{:S(2)}, u32[]{:S(2)}) %collective-permute-start.3) | collective-permute-done | bytes 262176 | tf_op jit(solution)/shard_map/ppermute | solution.py:53
  98.8 0.0 copy-start.3
  98.9 1.1 constant_dynamic-slice_fusion
  100.0 0.0 all-gather.11.cloned.1.call-update
  100.0 0.1 fusion.44
  100.1 30.5 %all-gather.9.cloned.1.call-done = bf16[2,2048,1024]{2,1,0:T(8,128)(2,1)} async-done(((bf16[2,2048,256]{2,1,0:T(8,128)(2,1)}), bf16[2,2048,1024]{2,1,0:T(8,128)(2,1)}) %all-gather.9.cloned.1.call-update) | async-done | bytes 8388624 | tf_op jit(solution)/shard_map/all_gather | solution.py:29
  130.6 8.1 %convert_bitcast_fusion = bf16[2,512,1024]{2,1,0:T(8,128)(2,1)S(1)} fusion(bf16[2,2048,1024]{2,1,0:T(8,128)(2,1)} %all-gather.9.cloned.1.call-done, bf16[1,512,2048]{2,1,0:T(8,128)(2,1)S(1)} %copy-done), kind=kOutput, calls=%fused_computation.68 | convolution fusion | flops 4296015872 | bytes 12582912 | tf_op jit(solution)/shard_map/td,kdc->ktc/dot_general | solution.py:26
  138.7 0.6 multiply_convert_fusion
  139.3 3.4 %collective-permute-start = (bf16[30,1024]{1,0:T(8,128)(2,1)S(1)}, bf16[30,1024]{1,0:T(8,128)(2,1)S(1)}, u32[]{:S(2)}, u32[]{:S(2)}) collective-permute-start(bf16[30,1024]{1,0:T(8,128)(2,1)S(1)} %slice_bitcast_fusion), channel_id=1, source_target_pairs={{0,4},{4,8},{8,12},{1,5},{5,9},{9,13},{2,6},{6,10},{10,14},{3,7},{... | collective-permute-start | bytes 184328 | tf_op jit(solution)/shard_map/ppermute | solution.py:12
  142.7 0.6 fusion.48
  143.3 1.3 collective-permute-done
  144.6 0.3 maximum_convert_fusion
  144.9 9.8 %fusion.42 = (f32[512]{0:T(512)S(1)}, f32[512,1024]{1,0:T(8,128)S(1)}) fusion(f32[542,1024]{1,0:T(8,128)S(1)} %maximum_convert_fusion, f32[1024]{0:T(1024)S(1)} %bitcast.61, f32[1024]{0:T(1024)S(1)} %bitcast.62, f32[1024]{0:T(1024)S(1)} %bitcast.64, f32[1024]{0:T(1024)S(1)} %bitcast.65, f32[1024]{0:T(1024)S(1)} %bitcast.66, f32[1024]{0:T(1024)S(1)} %bitcast.67, ...), kind=kLoop, calls=%fused_computation.90 | loop fusion | flops 33029632 | bytes 67241984 | tf_op jit(solution)/shard_map/reduce_sum | solution.py:46
  154.8 0.0 copy-start.5
  154.8 0.0 copy-start.6
  154.8 1.3 copy-done.1
  156.1 0.3 multiply_reduce_fusion
  156.4 10.1 %all-gather.11.cloned.1.call-done = bf16[1024,2048]{1,0:T(8,128)(2,1)} async-done(((bf16[1024,512]{1,0:T(8,128)(2,1)}), bf16[1024,2048]{1,0:T(8,128)(2,1)}) %all-gather.11.cloned.1.call-update) | async-done | bytes 4194320 | tf_op jit(solution)/shard_map/all_gather | solution.py:59
  166.5 7.0 %fusion = bf16[1,512,2048]{2,1,0:T(8,128)(2,1)} fusion(bf16[1024,2048]{1,0:T(8,128)(2,1)} %all-gather.11.cloned.1.call-done, f32[512,1024]{1,0:T(8,128)} %copy-done.1, f32[1024]{0:T(1024)S(1)} %copy-done.5, f32[1024]{0:T(1024)S(1)} %copy-done.6, f32[512]{0:T(512)S(1)} %add_rsqrt_fusion, f32[512]{0:T(512)S(1)} %broadcast_multiply_fusion), kind=kOutput, calls=%fused_computation.1 | convolution fusion | flops 2153250816 | bytes 8400896 | tf_op jit(solution)/shard_map/dot_general | solution.py:57
  (24 shorter events, 0.3 us)
Async XLA Ops:
  6.5 124.1 %copy-start = (bf16[1,512,2048]{2,1,0:T(8,128)(2,1)S(1)}, bf16[1,512,2048]{2,1,0:T(8,128)(2,1)}, u32[]{:S(2)}) copy-start(bf16[1,512,2048]{2,1,0:T(8,128)(2,1)} %param.8) | copy-start | bytes 6291460
  6.5 33.1 %all-gather.5.cloned.1.call-start = ((), (), s32[]{:S(2)}) async-start(), calls=%async_computation | async-start | bytes 1310720 | tf_op jit(solution)/shard_map/all_gather | solution.py:22
  7.3 61.3 %all-gather.7.cloned.1.call-start = ((), (), s32[]{:S(2)}) async-start(), calls=%async_computation.1 | async-start | bytes 1310720 | tf_op jit(solution)/shard_map/all_gather | solution.py:23
  8.0 122.6 %all-gather.9.cloned.1.call-start = ((), (), s32[]{:S(2)}) async-start(), calls=%async_computation.2 | async-start | bytes 10485760 | tf_op jit(solution)/shard_map/all_gather | solution.py:29
  71.7 0.9 copy-start.2
  71.7 94.8 %all-gather.11.cloned.1.call-start = ((), (), s32[]{:S(2)}) async-start(), calls=%async_computation.3 | async-start | bytes 5242880 | tf_op jit(solution)/shard_map/all_gather | solution.py:59
  72.6 9.4 %collective-permute-start.1 = (bf16[256,512]{1,0:T(8,128)(2,1)S(1)}, bf16[256,512]{1,0:T(8,128)(2,1)S(1)}, u32[]{:S(2)}, u32[]{:S(2)}) collective-permute-start(bf16[256,512]{1,0:T(8,128)(2,1)S(1)} %copy-done.2), channel_id=1, source_target_pairs={{0,4},{4,8},{8,12},{12,0},{1,5},{5,9},{9,13},{13,1},{2,6},{6,10},{... | collective-permute-start | bytes 786440 | tf_op jit(solution)/shard_map/ppermute | solution.py:53
  82.0 8.5 %collective-permute-start.2 = (bf16[256,512]{1,0:T(8,128)(2,1)S(1)}, bf16[256,512]{1,0:T(8,128)(2,1)S(1)}, u32[]{:S(2)}, u32[]{:S(2)}) collective-permute-start(bf16[256,512]{1,0:T(8,128)(2,1)S(1)} %collective-permute-done.1), channel_id=1, source_target_pairs={{0,4},{4,8},{8,12},{12,0},{1,5},{5,9},{9,13},{13,1},{2,6},{6,10},{... | collective-permute-start | bytes 786440 | tf_op jit(solution)/shard_map/ppermute | solution.py:53
  90.5 8.2 %collective-permute-start.3 = (bf16[256,512]{1,0:T(8,128)(2,1)S(1)}, bf16[256,512]{1,0:T(8,128)(2,1)S(1)}, u32[]{:S(2)}, u32[]{:S(2)}) collective-permute-start(bf16[256,512]{1,0:T(8,128)(2,1)S(1)} %collective-permute-done.2), channel_id=1, source_target_pairs={{0,4},{4,8},{8,12},{12,0},{1,5},{5,9},{9,13},{13,1},{2,6},{6,10},{... | collective-permute-start | bytes 786440 | tf_op jit(solution)/shard_map/ppermute | solution.py:53
  98.8 1.2 copy-start.3
  139.3 5.3 %collective-permute-start = (bf16[30,1024]{1,0:T(8,128)(2,1)S(1)}, bf16[30,1024]{1,0:T(8,128)(2,1)S(1)}, u32[]{:S(2)}, u32[]{:S(2)}) collective-permute-start(bf16[30,1024]{1,0:T(8,128)(2,1)S(1)} %slice_bitcast_fusion), channel_id=1, source_target_pairs={{0,4},{4,8},{8,12},{1,5},{5,9},{9,13},{2,6},{6,10},{10,14},{3,7},{... | collective-permute-start | bytes 184328 | tf_op jit(solution)/shard_map/ppermute | solution.py:12
  143.3 1.6 copy-start.4
  154.7 1.3 copy-start.1
  154.8 11.7 %copy-start.5 = (f32[1024]{0:T(1024)S(1)}, f32[1024]{0:T(1024)}, u32[]{:S(2)}) copy-start(f32[1024]{0:T(1024)} %param.14) | copy-start | bytes 12292
  154.8 11.7 %copy-start.6 = (f32[1024]{0:T(1024)S(1)}, f32[1024]{0:T(1024)}, u32[]{:S(2)}) copy-start(f32[1024]{0:T(1024)} %param.13) | copy-start | bytes 12292
Sparse Core Ops, SparseCore 0:
  8.9 30.6 all-gather.4
  41.2 27.3 all-gather.6
  71.8 58.7 all-gather.8
  132.0 34.4 all-gather.10
